TPU v7x, 32 devices: a whole 2x2x4 slice. The times are simulated.
32 devices in a mesh: fs: 16 (over z, y, x), tp: 2 (over core).
Axes of the slice: x: 2, y: 2, z: 4, core: 2. Of those that a mesh axis runs over, the one named last changes fastest.
Arguments:
- tokens: bfloat16 [6144, 2048], P('fs', 'tp'), may hold values from -24 to 24, as said below
- mixer_gain: float32 [2048], replicated, may hold values from 0.1 to 1.9
- w_content: float32 [2048, 1024], P('fs', 'tp'), may hold values from -0.125 to 0.125
- w_spatial: float32 [2048, 1024], P('fs', 'tp'), may hold values from -0.125 to 0.125
- content_scale: float32 [1024], P('tp'), may hold values from 0.5 to 2
- spatial_scale: float32 [1024], P('tp'), may hold values from 0.2 to 3.5, as said below
- spatial_gain: float32 [1024], P('tp'), may hold values from 0.1 to 1.9
- block_mixing: bfloat16 [8, 128, 128], P('tp'), may hold values from -0.5 to 0.5
- block_bias: float32 [8, 128], P('tp'), may hold values from -6 to 6
- w_project: float32 [1024, 2048], P('tp', 'fs'), may hold values from -0.1875 to 0.1875
- project_scale: float32 [2048], P('fs'), may hold values from 0.5 to 2
- channel_gain: float32 [2048], replicated, may hold values from 0.1 to 1.9
- w_up: float32 [2048, 8192], P('fs', 'tp'), may hold values from -0.125 to 0.125
- up_scale: float32 [8192], P('tp'), may hold values from 0.5 to 2
- w_down: float32 [8192, 2048], P('tp', 'fs'), may hold values from -0.0625 to 0.0625
- down_scale: float32 [2048], P('fs'), may hold values from 0.5 to 2
Outputs:
- layer_out: bfloat16 [6144, 2048], P('fs', 'tp')
Inputs may be any that keep to these rules, and one draw needn't show every extreme that they name: `tokens`: activations whose features and rows have differing scales. `spatial_scale`: positive column scales.
All inputs are finite; a program needn't handle non-finite values.
Results may differ from a plain program's by a relative error of at most 0.019.
Values may be sent and summed in bfloat16 or wider, within the bound.
A program may use at most 128 MiB of HBM per device.

v0:
```python
import jax
import jax.numpy as jnp
from jax import lax
from jax.sharding import PartitionSpec as P

EPSILON = 1e-06


def normalize_rows(token_rows, gain_vector):
    values = token_rows.astype(jnp.float32)
    scaled = values * lax.rsqrt(jnp.mean(values * values, axis=-1, keepdims=True) + EPSILON)
    return (scaled * gain_vector).astype(jnp.bfloat16)


def shards(
    tokens,
    mixer_gain,
    w_content,
    w_spatial,
    content_scale,
    spatial_scale,
    spatial_gain,
    block_mixing,
    block_bias,
    w_project,
    project_scale,
    channel_gain,
    w_up,
    up_scale,
    w_down,
    down_scale,
):
    content_weight = w_content.astype(jnp.bfloat16)
    spatial_weight = w_spatial.astype(jnp.bfloat16)
    project_weight = w_project.astype(jnp.bfloat16)
    up_weight = w_up.astype(jnp.bfloat16)
    down_weight = w_down.astype(jnp.bfloat16)
    project_full, down_full = (
        lax.all_gather(project_scale, "fs", axis=0, tiled=True),
        lax.all_gather(down_scale, "fs", axis=0, tiled=True),
    )
    gathered_rows = lax.all_gather(tokens, "tp", axis=1, tiled=True)
    normed = normalize_rows(gathered_rows, mixer_gain)
    row_count = gathered_rows.shape[0]
    content_full, spatial_full, project_cols = (
        lax.all_gather(content_weight, "fs", axis=0, tiled=True),
        lax.all_gather(spatial_weight, "fs", axis=0, tiled=True),
        lax.all_gather(project_weight, "fs", axis=1, tiled=True),
    )
    content_linear = jnp.dot(normed, content_full, preferred_element_type=jnp.float32)
    spatial_linear = jnp.dot(normed, spatial_full, preferred_element_type=jnp.float32)
    content = jax.nn.gelu(content_linear * content_scale)
    spatial = jax.nn.gelu(spatial_linear * spatial_scale)
    square_sums = lax.psum(jnp.sum(spatial * spatial, axis=1), "tp")
    total_width = spatial.shape[1] * lax.axis_size("tp")
    spatial_norm = (
        spatial * lax.rsqrt(square_sums / total_width + EPSILON)[:, None] * spatial_gain
    ).astype(jnp.bfloat16)
    groups_here = block_mixing.shape[0]
    block_size = block_mixing.shape[1]
    group_width = spatial_norm.shape[1] // groups_here
    causal_mask = jnp.tril(jnp.ones((block_size, block_size), dtype=bool))
    mixing_weights = jnp.where(causal_mask[None, :, :], block_mixing, jnp.zeros_like(block_mixing))
    grouped = spatial_norm.reshape(row_count // block_size, block_size, groups_here, group_width)
    mixed_block = (
        jnp.einsum("gts,nsgc->ntgc", mixing_weights, grouped, preferred_element_type=jnp.float32)
        + block_bias.T[None, :, :, None]
    )
    gated = (content * mixed_block.reshape(row_count, spatial_norm.shape[1])).astype(jnp.bfloat16)
    mixer_terms = jnp.dot(gated, project_cols, preferred_element_type=jnp.float32) * project_full
    mixer_sum = lax.psum_scatter(
        mixer_terms.astype(jnp.bfloat16), "tp", scatter_dimension=1, tiled=True
    ).astype(jnp.float32)
    middle = (tokens.astype(jnp.float32) + mixer_sum).astype(jnp.bfloat16)
    middle_rows = lax.all_gather(middle, "tp", axis=1, tiled=True)
    channel_normed = normalize_rows(middle_rows, channel_gain)
    up_full, down_cols = (
        lax.all_gather(up_weight, "fs", axis=0, tiled=True),
        lax.all_gather(down_weight, "fs", axis=1, tiled=True),
    )
    up_linear = jnp.dot(channel_normed, up_full, preferred_element_type=jnp.float32)
    hidden = jnp.square(jax.nn.relu(up_linear * up_scale)).astype(jnp.bfloat16)
    channel_terms = jnp.dot(hidden, down_cols, preferred_element_type=jnp.float32) * down_full
    channel_sum = lax.psum_scatter(
        channel_terms.astype(jnp.bfloat16), "tp", scatter_dimension=1, tiled=True
    ).astype(jnp.float32)
    return (middle.astype(jnp.float32) + channel_sum).astype(jnp.bfloat16)


def solution(mesh):
    return jax.shard_map(
        shards,
        mesh=mesh,
        in_specs=(
            P("fs", "tp"),
            P(),
            P("fs", "tp"),
            P("fs", "tp"),
            P("tp"),
            P("tp"),
            P("tp"),
            P("tp", None, None),
            P("tp", None),
            P("tp", "fs"),
            P("fs"),
            P(),
            P("fs", "tp"),
            P("tp"),
            P("tp", "fs"),
            P("fs"),
        ),
        out_specs=P("fs", "tp"),
        check_vma=False,
    )
```

profile of v0, /device:TPU:0, one launch (start us, length us, event | category | flops | bytes accessed | tf_op | source)
XLA Modules:
  0.0 725.1 jit_solution(8672027433226947679)
XLA Ops:
  6.5 0.7 all-gather.10.cloned.1.call-update
  7.3 1.6 convert_element_type.64
  9.0 1.7 convert_element_type.63
  10.8 1.6 convert_element_type.67
  12.5 42.4 %all-gather = f32[16,1,128]{2,1,0:T(1,128)S(1)} all-gather(f32[1,1,128]{2,1,0:T(1,128)S(1)} %bitcast.30), channel_id=1, replica_groups=mesh['fs'=16,'tp'=2] {'fs'}, dimensions={0}, use_global_device_ids=true | all-gather | bytes 8704 | tf_op jit(solution)/shard_map/all_gather | solution.py:39
  55.0 1.8 fusion.1
  56.8 29.0 %all-gather.14.cloned.1.call-done = bf16[2048,512]{1,0:T(8,128)(2,1)} async-done(((bf16[128,512]{1,0:T(8,128)(2,1)}), bf16[2048,512]{1,0:T(8,128)(2,1)}) %all-gather.14.cloned.1.call-update) | async-done | bytes 2097168 | tf_op jit(solution)/shard_map/all_gather | solution.py:47
  85.8 3.4 multiply_reduce_fusion
  89.2 2.5 psum.7
  92.0 0.3 fusion.15
  92.6 55.2 %all-gather.12.cloned.1.call-done = bf16[2048,512]{1,0:T(8,128)(2,1)} async-done(((bf16[128,512]{1,0:T(8,128)(2,1)}), bf16[2048,512]{1,0:T(8,128)(2,1)}) %all-gather.12.cloned.1.call-update) | async-done | bytes 2097168 | tf_op jit(solution)/shard_map/all_gather | solution.py:46
  147.8 64.3 %all-gather.16.cloned.1.call-done = bf16[512,2048]{1,0:T(8,128)(2,1)} async-done(((bf16[512,128]{1,0:T(8,128)(2,1)}), bf16[512,2048]{1,0:T(8,128)(2,1)}) %all-gather.16.cloned.1.call-update) | async-done | bytes 2097168 | tf_op jit(solution)/shard_map/all_gather | solution.py:48
  212.1 5.5 multiply_convert_fusion.2
  217.7 7.2 reduce-scatter.3.cloned.1.call-done
  224.9 2.3 add_convert_fusion.1
  227.3 1.1 convert_element_type.74
  228.5 2.7 convert_element_type.76
  231.3 41.9 %all-gather.1 = f32[16,1,128]{2,1,0:T(1,128)S(1)} all-gather(f32[1,1,128]{2,1,0:T(1,128)S(1)} %bitcast.31), channel_id=1, replica_groups=mesh['fs'=16,'tp'=2] {'fs'}, dimensions={0}, use_global_device_ids=true | all-gather | bytes 8704 | tf_op jit(solution)/shard_map/all_gather | solution.py:40
  273.2 1.8 fusion.4
  275.0 158.5 %all-gather.20.cloned.1.call-done = bf16[2048,4096]{1,0:T(8,128)(2,1)} async-done(((bf16[128,4096]{1,0:T(8,128)(2,1)}), bf16[2048,4096]{1,0:T(8,128)(2,1)}) %all-gather.20.cloned.1.call-update) | async-done | bytes 16777232 | tf_op jit(solution)/shard_map/all_gather | solution.py:78
  433.5 250.0 %all-gather.22.cloned.1.call-done = bf16[4096,2048]{1,0:T(8,128)(2,1)} async-done(((bf16[4096,128]{1,0:T(8,128)(2,1)}), bf16[4096,2048]{1,0:T(8,128)(2,1)}) %all-gather.22.cloned.1.call-update) | async-done | bytes 16777232 | tf_op jit(solution)/shard_map/all_gather | solution.py:79
  683.5 25.4 %multiply_convert_fusion.1 = bf16[384,2048]{1,0:T(8,128)(2,1)} fusion(bf16[4096,2048]{1,0:T(8,128)(2,1)} %all-gather.22.cloned.1.call-done, bf16[2048,4096]{1,0:T(8,128)(2,1)} %all-gather.20.cloned.1.call-done, f32[4096]{0:T(1024)S(1)} %copy-done.9, bf16[384,2048]{1,0:T(8,128)(2,1)} %all-gather.18.cloned.1.call-done, f32[2048]{0:T(1024)S(1)} %bitcast.28, ...), kind=kOutput, calls=%fused_computation.12 | convolution fusion | flops 12895911936 | bytes 36734464 | tf_op jit(solution)/shard_map/dot_general | solution.py:83
  708.9 7.3 %reduce-scatter.5.cloned.1.call-done = bf16[384,1024]{1,0:T(8,128)(2,1)} async-done(((bf16[384,2048]{1,0:T(8,128)(2,1)}), bf16[384,1024]{1,0:T(8,128)(2,1)}) %reduce-scatter.5.cloned.1.call-update) | async-done | bytes 786448 | tf_op jit(solution)/shard_map/reduce_scatter | solution.py:84
  716.2 2.3 add_convert_fusion
  (54 shorter events, 1.1 us)
Async XLA Ops:
  6.5 5.9 copy-start.7
  6.5 79.3 %copy-start.10 = (f32[2048]{0:T(1024)S(1)}, f32[2048]{0:T(1024)}, u32[]{:S(2)}) copy-start(f32[2048]{0:T(1024)} %param.17) | copy-start | bytes 24580
  6.5 79.3 %copy-start.12 = (f32[512]{0:T(512)S(1)}, f32[512]{0:T(512)}, u32[]{:S(2)}) copy-start(f32[512]{0:T(512)} %param.21) | copy-start | bytes 6148
  6.5 48.4 %all-gather.10.cloned.1.call-start = ((), (), s32[]{:S(2)}) async-start(), calls=%async_computation.2 | async-start | bytes 2359296 | tf_op jit(solution)/shard_map/all_gather | solution.py:42
  7.3 78.5 %all-gather.14.cloned.1.call-start = ((), (), s32[]{:S(2)}) async-start(), calls=%async_computation.4 | async-start | bytes 2228224 | tf_op jit(solution)/shard_map/all_gather | solution.py:47
  9.0 138.8 %all-gather.12.cloned.1.call-start = ((), (), s32[]{:S(2)}) async-start(), calls=%async_computation.3 | async-start | bytes 2228224 | tf_op jit(solution)/shard_map/all_gather | solution.py:46
  10.7 201.4 %all-gather.16.cloned.1.call-start = ((), (), s32[]{:S(2)}) async-start(), calls=%async_computation.5 | async-start | bytes 2228224 | tf_op jit(solution)/shard_map/all_gather | solution.py:48
  12.4 212.5 %reduce-scatter.3.cloned.1.call-start = ((), (), s32[]{:S(2)}) async-start(), calls=%async_computation.6 | async-start | bytes 2359296 | tf_op jit(solution)/shard_map/reduce_scatter | solution.py:71
  56.8 34.9 %copy-start.5 = (f32[512]{0:T(512)S(1)}, f32[512]{0:T(512)}, u32[]{:S(2)}) copy-start(f32[512]{0:T(512)} %param.22) | copy-start | bytes 6148
  56.8 35.2 %copy-start.4 = (bf16[4,128,128]{2,1,0:T(8,128)(2,1)S(1)}, bf16[4,128,128]{2,1,0:T(8,128)(2,1)}, u32[]{:S(2)}) copy-start(bf16[4,128,128]{2,1,0:T(8,128)(2,1)} %param.23) | copy-start | bytes 393220
  56.8 35.2 %copy-start.6 = (f32[4,128]{1,0:T(4,128)S(1)}, f32[4,128]{1,0:T(4,128)}, u32[]{:S(2)}) copy-start(f32[4,128]{1,0:T(4,128)} %param.24) | copy-start | bytes 6148
  91.8 120.3 %copy-start.3 = (bf16[384,2048]{1,0:T(8,128)(2,1)S(1)}, bf16[384,2048]{1,0:T(8,128)(2,1)}, u32[]{:S(2)}) copy-start(bf16[384,2048]{1,0:T(8,128)(2,1)} %all-gather.10.cloned.1.call-done) | copy-start | bytes 4718596
  91.8 120.3 %copy-start.13 = (f32[512]{0:T(512)S(1)}, f32[512]{0:T(512)}, u32[]{:S(2)}) copy-start(f32[512]{0:T(512)} %param.20) | copy-start | bytes 6148
  217.6 7.3 %copy-start.1 = (bf16[384,1024]{1,0:T(8,128)(2,1)S(1)}, bf16[384,1024]{1,0:T(8,128)(2,1)}, u32[]{:S(2)}) copy-start(bf16[384,1024]{1,0:T(8,128)(2,1)} %param.16) | copy-start | bytes 2359300
  217.6 9.7 %copy-start.2 = (f32[128,4096]{1,0:T(8,128)S(1)}, f32[128,4096]{1,0:T(8,128)}, u32[]{:S(2)}) copy-start(f32[128,4096]{1,0:T(8,128)} %param.28) | copy-start | bytes 6291460
  217.6 55.5 %all-gather.18.cloned.1.call-start = ((), (), s32[]{:S(2)}) async-start(), calls=%async_computation.7 | async-start | bytes 2359296 | tf_op jit(solution)/shard_map/all_gather | solution.py:75
  227.3 206.2 %all-gather.20.cloned.1.call-start = ((), (), s32[]{:S(2)}) async-start(), calls=%async_computation.8 | async-start | bytes 17825792 | tf_op jit(solution)/shard_map/all_gather | solution.py:78
  228.5 2.8 copy-start.8
  228.5 455.1 %all-gather.22.cloned.1.call-start = ((), (), s32[]{:S(2)}) async-start(), calls=%async_computation.9 | async-start | bytes 17825792 | tf_op jit(solution)/shard_map/all_gather | solution.py:79
  231.2 452.3 %copy-start.9 = (f32[4096]{0:T(1024)S(1)}, f32[4096]{0:T(1024)}, u32[]{:S(2)}) copy-start(f32[4096]{0:T(1024)} %param.29) | copy-start | bytes 49156
  231.2 452.3 %copy-start.11 = (f32[2048]{0:T(1024)S(1)}, f32[2048]{0:T(1024)}, u32[]{:S(2)}) copy-start(f32[2048]{0:T(1024)} %param.27) | copy-start | bytes 24580
  231.3 485.0 %reduce-scatter.5.cloned.1.call-start = ((), (), s32[]{:S(2)}) async-start(), calls=%async_computation.10 | async-start | bytes 2359296 | tf_op jit(solution)/shard_map/reduce_scatter | solution.py:84
  708.9 7.3 %copy-start = (bf16[384,1024]{1,0:T(8,128)(2,1)S(1)}, bf16[384,1024]{1,0:T(8,128)(2,1)}, u32[]{:S(2)}) copy-start(bf16[384,1024]{1,0:T(8,128)(2,1)} %add_convert_fusion.1) | copy-start | bytes 2359300
Sparse Core Ops, SparseCore 0:
  8.9 12.5 all-gather.9
  24.2 61.5 all-gather.13
  88.6 59.1 all-gather.11
  150.3 61.7 all-gather.15
  217.8 7.1 reduce-scatter.2
  227.4 11.0 all-gather.17
  241.3 192.1 all-gather.19
  436.2 247.2 all-gather.21
  709.1 7.1 reduce-scatter.4
where the time goes:
time: 726 us; the launch traced here: 725 us
  waiting for transfers between devices  572 us (79%)
  blocking collectives  86.8 us (12%)
  matrix products  34.6 us (5%)
  other arithmetic  17.1 us (2%)
  between operations  13.3 us (2%)
    all_gather x1, waiting for transfers between devices, shards(): lax.all_gather(down_weight, 'fs', axis=1, tiled=True)  250 us
    all_gather x1, waiting for transfers between devices, shards(): lax.all_gather(up_weight, 'fs', axis=0, tiled=True)  159 us
    all_gather x1, waiting for transfers between devices, shards(): lax.all_gather(project_weight, 'fs', axis=1, tiled=True)  64.3 us
    all_gather x1, waiting for transfers between devices, shards(): lax.all_gather(content_weight, 'fs', axis=0, tiled=True)  55.2 us
    all_gather x1, blocking collectives, shards(): lax.all_gather(project_scale, 'fs', axis=0, tiled=True)  42.4 us
    all_gather x1, blocking collectives, shards(): lax.all_gather(down_scale, 'fs', axis=0, tiled=True)  41.9 us
    all_gather x1, waiting for transfers between devices, shards(): lax.all_gather(spatial_weight, 'fs', axis=0, tiled=True)  29 us
    dot_general x1, matrix products, shards(): jnp.dot(hidden, down_cols, preferred_element_type=jnp.float32) * down_full  25.4 us
  transfers between devices with their start and end apart: 9, of which 7 were waited for; matrix products, arithmetic and copies ran while one was open for 2% of the time, Pallas kernels for 0%

commit v1 on v0

--- a/solution.py
+++ b/solution.py
@@ -76,7 +76,7 @@
     channel_normed = normalize_rows(middle_rows, channel_gain)
     up_full, down_cols = (
         lax.all_gather(up_weight, "fs", axis=0, tiled=True),
-        lax.all_gather(down_weight, "fs", axis=1, tiled=True),
+        jnp.concatenate(lax.all_gather(down_weight, "fs"), axis=1),
     )
     up_linear = jnp.dot(channel_normed, up_full, preferred_element_type=jnp.float32)
     hidden = jnp.square(jax.nn.relu(up_linear * up_scale)).astype(jnp.bfloat16)

time: 726 us -> 662 us (0.912)
  waiting for transfers between devices: 572 us -> 493 us
  local copies, waits for them, and re-layouts: 0.48 us -> 21.6 us
    all_gather x1, waiting for transfers between devices: 250 us -> 159 us  [shards(): lax.all_gather(down_weight, 'fs')]
    reshape x0 -> x1, local copies, waits for them, and re-layouts: none -> 21.1 us  [shards(): jnp.concatenate(lax.all_gather(down_weight, 'fs'), axis=1)]
    all_gather x1, waiting for transfers between devices: 159 us -> 171 us  [shards(): lax.all_gather(up_weight, 'fs', axis=0, tiled=True)]
  transfers between devices with their start and end apart: 9 -> 9, of which waited for: 7 -> 7; matrix products, arithmetic and copies ran while one was open for 2% -> 6% of each run, Pallas kernels for 0% -> 0%
where the time goes in v1:
time: 662 us; the launch traced here: 661 us
  waiting for transfers between devices  493 us (74%)
  blocking collectives  86.8 us (13%)
  matrix products  28.6 us (4%)
  local copies, waits for them, and re-layouts  21.6 us (3%)
  other arithmetic  17.1 us (3%)
  between operations  13.3 us (2%)
    all_gather x1, waiting for transfers between devices, shards(): lax.all_gather(up_weight, 'fs', axis=0, tiled=True)  171 us
    all_gather x1, waiting for transfers between devices, shards(): lax.all_gather(down_weight, 'fs')  159 us
    all_gather x1, waiting for transfers between devices, shards(): lax.all_gather(project_weight, 'fs', axis=1, tiled=True)  64.3 us
    all_gather x1, waiting for transfers between devices, shards(): lax.all_gather(content_weight, 'fs', axis=0, tiled=True)  55.2 us
    all_gather x1, blocking collectives, shards(): lax.all_gather(project_scale, 'fs', axis=0, tiled=True)  42.6 us
    all_gather x1, blocking collectives, shards(): lax.all_gather(down_scale, 'fs', axis=0, tiled=True)  41.7 us
    all_gather x1, waiting for transfers between devices, shards(): lax.all_gather(spatial_weight, 'fs', axis=0, tiled=True)  28.9 us
    reshape x1, local copies, waits for them, and re-layouts, shards(): jnp.concatenate(lax.all_gather(down_weight, 'fs'), axis=1)  21.1 us
  transfers between devices with their start and end apart: 9, of which 7 were waited for; matrix products, arithmetic and copies ran while one was open for 6% of the time, Pallas kernels for 0%

profile of v1, /device:TPU:0, one launch (start us, length us, event | category | flops | bytes accessed | tf_op | source)
XLA Modules:
  0.0 661.1 jit_solution(17727143611421885555)
XLA Ops:
  6.5 0.7 all-gather.11.cloned.1.call-update
  7.3 1.6 convert_element_type.64
  9.0 1.6 convert_element_type.63
  10.7 1.6 convert_element_type.67
  12.4 42.6 %all-gather.1 = f32[16,1,128]{2,1,0:T(1,128)S(1)} all-gather(f32[1,1,128]{2,1,0:T(1,128)} %bitcast.36), channel_id=1, replica_groups=mesh['fs'=16,'tp'=2] {'fs'}, dimensions={0}, use_global_device_ids=true | all-gather | bytes 8704 | tf_op jit(solution)/shard_map/all_gather | solution.py:39
  55.1 1.8 fusion
  56.9 28.9 %all-gather.15.cloned.1.call-done = bf16[2048,512]{1,0:T(8,128)(2,1)} async-done(((bf16[128,512]{1,0:T(8,128)(2,1)}), bf16[2048,512]{1,0:T(8,128)(2,1)}) %all-gather.15.cloned.1.call-update) | async-done | bytes 2097168 | tf_op jit(solution)/shard_map/all_gather | solution.py:47
  85.8 3.4 multiply_reduce_fusion
  89.2 2.5 psum.7
  92.6 55.2 %all-gather.13.cloned.1.call-done = bf16[2048,512]{1,0:T(8,128)(2,1)} async-done(((bf16[128,512]{1,0:T(8,128)(2,1)}), bf16[2048,512]{1,0:T(8,128)(2,1)}) %all-gather.13.cloned.1.call-update) | async-done | bytes 2097168 | tf_op jit(solution)/shard_map/all_gather | solution.py:46
  147.8 64.3 %all-gather.17.cloned.1.call-done = bf16[512,2048]{1,0:T(8,128)(2,1)} async-done(((bf16[512,128]{1,0:T(8,128)(2,1)}), bf16[512,2048]{1,0:T(8,128)(2,1)}) %all-gather.17.cloned.1.call-update) | async-done | bytes 2097168 | tf_op jit(solution)/shard_map/all_gather | solution.py:48
  212.1 6.0 multiply_convert_fusion.2
  218.2 7.2 %reduce-scatter.3.cloned.1.call-done = bf16[384,1024]{1,0:T(8,128)(2,1)} async-done(((bf16[384,2048]{1,0:T(8,128)(2,1)}), bf16[384,1024]{1,0:T(8,128)(2,1)}) %reduce-scatter.3.cloned.1.call-update) | async-done | bytes 786448 | tf_op jit(solution)/shard_map/reduce_scatter | solution.py:71
  225.5 2.3 add_convert_fusion.1
  227.9 1.1 convert_element_type.76
  229.1 2.7 convert_element_type.74
  231.8 41.7 %all-gather.2 = f32[16,1,128]{2,1,0:T(1,128)S(1)} all-gather(f32[1,1,128]{2,1,0:T(1,128)S(1)} %bitcast.37), channel_id=1, replica_groups=mesh['fs'=16,'tp'=2] {'fs'}, dimensions={0}, use_global_device_ids=true | all-gather | bytes 8704 | tf_op jit(solution)/shard_map/all_gather | solution.py:40
  273.6 1.8 fusion.3
  275.4 158.7 %all-gather.23.cloned.1.call-done = bf16[65536,128]{1,0:T(8,128)(2,1)} async-done(((bf16[4096,128]{1,0:T(8,128)(2,1)}), bf16[65536,128]{1,0:T(8,128)(2,1)}) %all-gather.23.cloned.1.call-update) | async-done | bytes 16777232 | tf_op jit(solution)/shard_map/all_gather | solution.py:79
  434.1 21.1 %copy.26 = bf16[4096,16,128]{0,2,1:T(8,128)(2,1)} copy(bf16[4096,16,128]{2,0,1:T(8,128)(2,1)} %bitcast.30) | data formatting | bytes 33554432 | tf_op jit(solution)/shard_map/reshape | solution.py:79
  455.2 170.9 %all-gather.21.cloned.1.call-done = bf16[2048,4096]{1,0:T(8,128)(2,1)} async-done(((bf16[128,4096]{1,0:T(8,128)(2,1)}), bf16[2048,4096]{1,0:T(8,128)(2,1)}) %all-gather.21.cloned.1.call-update) | async-done | bytes 16777232 | tf_op jit(solution)/shard_map/all_gather | solution.py:78
  626.1 18.9 %multiply_convert_fusion.1 = bf16[384,2048]{1,0:T(8,128)(2,1)} fusion(bf16[4096,2048]{0,1:T(8,128)(2,1)} %bitcast.31, bf16[2048,4096]{1,0:T(8,128)(2,1)} %all-gather.21.cloned.1.call-done, f32[4096]{0:T(1024)S(1)} %copy-done.8, bf16[384,2048]{1,0:T(8,128)(2,1)S(1)} %copy-done.3, f32[2048]{0:T(1024)S(1)} %bitcast.34, f32[2048]{0:T(1024)S(1)} %copy-done.10, ...), kind=kOutput, calls=%fused_computation.11 | convolution fusion | flops 12895911936 | bytes 36734464 | tf_op jit(solution)/shard_map/dot_general | solution.py:83
  645.0 7.3 %reduce-scatter.5.cloned.1.call-done = bf16[384,1024]{1,0:T(8,128)(2,1)} async-done(((bf16[384,2048]{1,0:T(8,128)(2,1)}), bf16[384,1024]{1,0:T(8,128)(2,1)}) %reduce-scatter.5.cloned.1.call-update) | async-done | bytes 786448 | tf_op jit(solution)/shard_map/reduce_scatter | solution.py:84
  652.2 2.3 add_convert_fusion
  (53 shorter events, 1.5 us)
Async XLA Ops:
  6.5 79.3 %copy-start.9 = (f32[2048]{0:T(1024)S(1)}, f32[2048]{0:T(1024)}, u32[]{:S(2)}) copy-start(f32[2048]{0:T(1024)} %param.17) | copy-start | bytes 24580
  6.5 79.3 %copy-start.11 = (f32[512]{0:T(512)S(1)}, f32[512]{0:T(512)}, u32[]{:S(2)}) copy-start(f32[512]{0:T(512)} %param.21) | copy-start | bytes 6148
  6.5 48.5 %all-gather.11.cloned.1.call-start = ((), (), s32[]{:S(2)}) async-start(), calls=%async_computation.2 | async-start | bytes 2359296 | tf_op jit(solution)/shard_map/all_gather | solution.py:42
  7.3 78.5 %all-gather.15.cloned.1.call-start = ((), (), s32[]{:S(2)}) async-start(), calls=%async_computation.4 | async-start | bytes 2228224 | tf_op jit(solution)/shard_map/all_gather | solution.py:47
  9.0 138.8 %all-gather.13.cloned.1.call-start = ((), (), s32[]{:S(2)}) async-start(), calls=%async_computation.3 | async-start | bytes 2228224 | tf_op jit(solution)/shard_map/all_gather | solution.py:46
  10.7 201.4 %all-gather.17.cloned.1.call-start = ((), (), s32[]{:S(2)}) async-start(), calls=%async_computation.5 | async-start | bytes 2228224 | tf_op jit(solution)/shard_map/all_gather | solution.py:48
  12.4 213.1 %reduce-scatter.3.cloned.1.call-start = ((), (), s32[]{:S(2)}) async-start(), calls=%async_computation.6 | async-start | bytes 2359296 | tf_op jit(solution)/shard_map/reduce_scatter | solution.py:71
  56.9 34.8 %copy-start.5 = (f32[512]{0:T(512)S(1)}, f32[512]{0:T(512)}, u32[]{:S(2)}) copy-start(f32[512]{0:T(512)} %param.22) | copy-start | bytes 6148
  56.9 35.0 %copy-start.4 = (bf16[4,128,128]{2,1,0:T(8,128)(2,1)S(1)}, bf16[4,128,128]{2,1,0:T(8,128)(2,1)}, u32[]{:S(2)}) copy-start(bf16[4,128,128]{2,1,0:T(8,128)(2,1)} %param.23) | copy-start | bytes 393220
  56.9 35.0 %copy-start.6 = (f32[4,128]{1,0:T(4,128)S(1)}, f32[4,128]{1,0:T(4,128)}, u32[]{:S(2)}) copy-start(f32[4,128]{1,0:T(4,128)} %param.24) | copy-start | bytes 6148
  89.2 122.9 %copy-start.12 = (f32[512]{0:T(512)S(1)}, f32[512]{0:T(512)}, u32[]{:S(2)}) copy-start(f32[512]{0:T(512)} %param.20) | copy-start | bytes 6148
  212.1 13.4 %copy-start.1 = (bf16[384,1024]{1,0:T(8,128)(2,1)S(1)}, bf16[384,1024]{1,0:T(8,128)(2,1)}, u32[]{:S(2)}) copy-start(bf16[384,1024]{1,0:T(8,128)(2,1)} %param.16) | copy-start | bytes 2359300
  218.2 9.7 %copy-start.2 = (f32[4096,128]{1,0:T(8,128)S(1)}, f32[4096,128]{1,0:T(8,128)}, u32[]{:S(2)}) copy-start(f32[4096,128]{1,0:T(8,128)} %param.30) | copy-start | bytes 6291460
  218.2 55.4 %all-gather.19.cloned.1.call-start = ((), (), s32[]{:S(2)}) async-start(), calls=%async_computation.7 | async-start | bytes 2359296 | tf_op jit(solution)/shard_map/all_gather | solution.py:75
  227.8 206.2 %all-gather.23.cloned.1.call-start = ((), (), s32[]{:S(2)}) async-start(), calls=%async_computation.10 | async-start | bytes 17825792 | tf_op jit(solution)/shard_map/all_gather | solution.py:79
  229.0 2.8 copy-start.7
  229.0 397.0 %all-gather.21.cloned.1.call-start = ((), (), s32[]{:S(2)}) async-start(), calls=%async_computation.8 | async-start | bytes 17825792 | tf_op jit(solution)/shard_map/all_gather | solution.py:78
  231.8 420.5 %reduce-scatter.5.cloned.1.call-start = ((), (), s32[]{:S(2)}) async-start(), calls=%async_computation.9 | async-start | bytes 2359296 | tf_op jit(solution)/shard_map/reduce_scatter | solution.py:84
  434.1 192.0 %copy-start.3 = (bf16[384,2048]{1,0:T(8,128)(2,1)S(1)}, bf16[384,2048]{1,0:T(8,128)(2,1)}, u32[]{:S(2)}) copy-start(bf16[384,2048]{1,0:T(8,128)(2,1)} %all-gather.19.cloned.1.call-done) | copy-start | bytes 4718596
  434.1 192.0 %copy-start.8 = (f32[4096]{0:T(1024)S(1)}, f32[4096]{0:T(1024)}, u32[]{:S(2)}) copy-start(f32[4096]{0:T(1024)} %param.29) | copy-start | bytes 49156
  434.1 192.0 %copy-start.10 = (f32[2048]{0:T(1024)S(1)}, f32[2048]{0:T(1024)}, u32[]{:S(2)}) copy-start(f32[2048]{0:T(1024)} %param.27) | copy-start | bytes 24580
  626.1 26.2 %copy-start = (bf16[384,1024]{1,0:T(8,128)(2,1)S(1)}, bf16[384,1024]{1,0:T(8,128)(2,1)}, u32[]{:S(2)}) copy-start(bf16[384,1024]{1,0:T(8,128)(2,1)} %add_convert_fusion.1) | copy-start | bytes 2359300
Sparse Core Ops, SparseCore 0:
  8.9 12.5 all-gather.10
  24.2 61.5 all-gather.14
  88.6 59.1 all-gather.12
  150.3 61.7 all-gather.16
  218.3 7.1 reduce-scatter.2
  227.9 11.0 all-gather.18
  241.8 192.1 all-gather.22
  436.8 189.1 all-gather.20
  645.1 7.1 reduce-scatter.4
